TPU v7x, 32 devices: a whole 2x2x4 slice. The times are simulated.
32 devices in a mesh: rep: 2 (over y), fs: 4 (over z), tp: 4 (over x, core).
Axes of the slice: x: 2, y: 2, z: 4, core: 2. Of those that a mesh axis runs over, the one named last changes fastest.
Arguments:
- out_grad: bfloat16 [2048, 2048], P(('rep', 'fs'), 'tp'), may hold values from -6 to 6
- gate_lin: bfloat16 [2048, 5632], P(('rep', 'fs'), 'tp'), may hold values from -6 to 6
- up_lin: bfloat16 [2048, 5632], P(('rep', 'fs'), 'tp'), may hold values from -6 to 6
- conv_weight: bfloat16 [3, 5632], replicated, may hold values from -3.5 to 3.5
- gate_weight: bfloat16 [2048, 5632], P('fs', 'tp'), may hold values from -0.125 to 0.125
- up_weight: bfloat16 [2048, 5632], P('fs', 'tp'), may hold values from -0.125 to 0.125
- down_weight: bfloat16 [5632, 2048], P('tp', 'fs'), may hold values from -0.078125 to 0.078125
Outputs:
- input_grad: bfloat16 [2048, 2048], P(('rep', 'fs'), 'tp')
- conv_grad: float32 [3, 5632], replicated
All inputs are finite; a program needn't handle non-finite values.
Results may differ from a plain program's by a relative error of at most 0.015.
Values may be sent and summed in bfloat16 or wider, within the bound.
A program may use at most 64 MiB of HBM per device.

v0:
```python
import math

import jax
import jax.numpy as jnp
from jax import lax
from jax.experimental import pallas as pl
from jax.experimental.pallas import tpu as pltpu
from jax.sharding import PartitionSpec as P


def extended(value, sides, width):
    for axis, dim in sides:
        peers, length = (lax.axis_size(axis), value.shape[dim])
        up = [(i, (i + 1) % peers) for i in range(peers - 1)]
        down = [(j, i) for i, j in up]
        last = lax.slice_in_dim(value, length - width, length, axis=dim)
        leading = lax.slice_in_dim(value, 0, width, axis=dim)
        before = lax.ppermute(last, axis, up)
        after = lax.ppermute(leading, axis, down)
        value = jnp.concatenate([before, value, after], axis=dim)
    return value


def gelu_parts(gate):
    normal_cdf = 0.5 * (1.0 + jax.scipy.special.erf(gate * (1.0 / math.sqrt(2.0))))
    density = jnp.exp(-0.5 * gate * gate) * (1.0 / math.sqrt(2.0 * math.pi))
    return (gate * normal_cdf, normal_cdf + gate * density)


def local(out_grad, gate_lin, up_lin, conv_weight, gate_weight, up_weight, down_weight):
    conv_full = conv_weight.astype(jnp.float32)
    column_count = gate_lin.shape[1]
    column_start = lax.axis_index("tp") * column_count
    conv_taps = lax.dynamic_slice_in_dim(conv_full, column_start, column_count, 1)
    grad_rows = lax.all_gather(out_grad, "tp", axis=1, tiled=True)
    act_grad = lax.dot_general(
        grad_rows,
        lax.all_gather(down_weight, "fs", axis=1, tiled=True),
        (((1,), (1,)), ((), ())),
        preferred_element_type=jnp.float32,
    )
    linear_mid = extended(gate_lin, (("fs", 0),), 1).astype(jnp.float32)
    gate = (
        conv_taps[0] * linear_mid[:-2]
        + conv_taps[1] * linear_mid[1:-1]
        + conv_taps[2] * linear_mid[2:]
    )
    gelu_value, gelu_slope = gelu_parts(gate)
    gate_grad = act_grad * up_lin.astype(jnp.float32) * gelu_slope
    grad_ext = extended(gate_grad.astype(jnp.bfloat16), (("fs", 0),), 1).astype(gate_grad.dtype)
    up_grad = (act_grad * gelu_value).astype(jnp.bfloat16)
    own_grad = grad_ext[1:-1]
    linear_grad = (
        conv_taps[0] * grad_ext[2:] + conv_taps[1] * own_grad + conv_taps[2] * grad_ext[:-2]
    ).astype(jnp.bfloat16)
    local_conv = jnp.stack(
        [
            jnp.sum(own_grad * linear_mid[:-2], axis=0),
            jnp.sum(own_grad * linear_mid[1:-1], axis=0),
            jnp.sum(own_grad * linear_mid[2:], axis=0),
        ]
    )
    product = lax.dot_general(
        linear_grad,
        lax.all_gather(gate_weight, "fs", axis=0, tiled=True),
        (((1,), (1,)), ((), ())),
        preferred_element_type=jnp.float32,
    )
    product = product + lax.dot_general(
        up_grad,
        lax.all_gather(up_weight, "fs", axis=0, tiled=True),
        (((1,), (1,)), ((), ())),
        preferred_element_type=jnp.float32,
    )
    input_grad = lax.psum_scatter(
        product.astype(jnp.bfloat16), "tp", scatter_dimension=1, tiled=True
    )
    summed_conv = lax.psum(local_conv, ("rep", "fs"))
    conv_grad = lax.all_gather(summed_conv, "tp", axis=1, tiled=True)
    return (input_grad, conv_grad)


EDGE = 16
PARTS = 4


def rows_dot(a, b):
    return lax.dot_general(a, b, (((1,), (1,)), ((), ())), preferred_element_type=jnp.float32)


def remote(src, dst, send, recv, device):
    return pltpu.make_async_remote_copy(
        src_ref=src,
        dst_ref=dst,
        send_sem=send,
        recv_sem=recv,
        device_id=device,
        device_id_type=pl.DeviceIdType.MESH,
    )


def arrived(dst, sem):
    pltpu.make_async_copy(dst, dst, sem).wait()


def kernel(
    og, gl, ul, cw, gw, uw, dw, out, cg,
    og_all, gl_all, ul_all, act, up_all, lin_all, wd, wg, wu,
    stage, parts_in, conv_own, conv_mid, conv_all,
    r_og, r_far, r_edge, l_far, l_edge, r_gl, r_ul, r_w, r_out, r_mid, r_conv,
    s_og, s_far, s_edge, s_gl, s_ul, s_hand, s_w, s_out, s_mid, s_conv,
):
    f32, bf16 = jnp.float32, jnp.bfloat16
    y, z, t = (lax.axis_index(a) for a in ("rep", "fs", "tp"))
    rows, width = og.shape
    hid = gl.shape[1]
    n_rows = 2 * rows + 2 * EDGE
    x = t // 2
    core = t % 2
    inner_z = 1 + z // 2
    outer_z = 3 * (z // 2)
    mid_z = 3 - inner_z
    base_z = 2 * (z // 2)
    twin = 2 * x + 1 - core
    relay_t = 2 * x + 1 - y
    lead = core == y
    inner = z == inner_z
    is_worker = jnp.logical_and(inner, lead)
    is_relay = jnp.logical_and(inner, core != y)
    is_outer = z != inner_z

    def block_rows(level):
        return pl.ds(pl.multiple_of(EDGE + (level % 2) * rows, EDGE), rows)

    def edge_rows(level):
        return pl.ds(pl.multiple_of((2 - level) * (EDGE + 2 * rows), EDGE), EDGE)

    edge_src = pl.ds(pl.multiple_of((2 - inner_z) * (rows - EDGE), EDGE), EDGE)

    def worker(block, level):
        return (block % 2, level, block)

    barrier = pltpu.get_barrier_semaphore()
    ts = (t, twin, (t + 2) % 4, (twin + 2) % 4)
    for a in range(2):
        for b in range(2):
            for d in range(4):
                if a or b or d:
                    level = z if b == 0 else base_z + 1 - z % 2
                    pl.semaphore_signal(
                        barrier,
                        inc=1,
                        device_id=((y + a) % 2, level, ts[d]),
                        device_id_type=pl.DeviceIdType.MESH,
                    )

    @pl.when(inner)
    def _():
        for a in range(2):
            for d in range(4):
                pl.semaphore_signal(
                    barrier,
                    inc=1,
                    device_id=((y + a) % 2, mid_z, ts[d]),
                    device_id_type=pl.DeviceIdType.MESH,
                )
        pl.semaphore_wait(barrier, 23)

    @pl.when(is_outer)
    def _():
        pl.semaphore_wait(barrier, 15)

    def w_slot(kind, level, part):
        buffer, size = ((wd, hid), (wg, width), (wu, width))[kind]
        size = size // PARTS
        return buffer.at[level, pl.ds(part * size, size), :]

    def w_src(kind, part):
        ref, size = ((dw, hid), (gw, width), (uw, width))[kind]
        size = size // PARTS
        return ref.at[pl.ds(part * size, size), :]

    order = [(0, p) for p in range(PARTS)] + [(k, p) for p in range(PARTS) for k in (1, 2)]

    def w_sem(kind, role, part):
        return (kind * 4 + role) * PARTS + part

    def saved_home():
        goal = worker(t, inner_z)
        kind = jnp.where(inner, 0, 1)
        slot = block_rows(z)
        return [
            remote(gl, gl_all.at[y, slot, :], s_gl.at[0], r_gl.at[y * 3 + kind], goal),
            remote(ul, ul_all.at[y, slot, :], s_ul.at[0], r_ul.at[y * 3 + kind], goal),
        ]

    def saved_edge():
        goal = worker(t, mid_z)
        slot = edge_rows(mid_z)
        return [
            remote(
                gl.at[edge_src, :], gl_all.at[y, slot, :], s_gl.at[1], r_gl.at[y * 3 + 2], goal
            ),
            remote(
                ul.at[edge_src, :], ul_all.at[y, slot, :], s_ul.at[1], r_ul.at[y * 3 + 2], goal
            ),
        ]

    def grad_edge():
        return [
            remote(
                og.at[edge_src, :],
                og_all.at[y, t, edge_rows(mid_z), :],
                s_edge.at[0],
                l_edge.at[core],
                (y, mid_z, relay_t),
            )
        ]

    def grad_own(block):
        return remote(
            og, og_all.at[y, t, block_rows(z), :], s_og.at[block], r_og.at[y * 4 + t],
            worker(block, z),
        )

    def grad_outer():
        return [
            remote(
                og,
                og_all.at[y, t, block_rows(z), :],
                s_hand.at[0],
                l_far.at[core],
                (y, inner_z, relay_t),
            )
        ]

    def pair(slot):
        return og_all.at[y, pl.ds(2 * x, 2), slot, :]

    def relay_edge(block):
        piece = pair(edge_rows(z))
        return remote(
            piece, piece, s_far.at[block], r_edge.at[y * 2 + x], worker(block, z)
        )

    def relay_outer(block):
        piece = pair(block_rows(outer_z))
        return remote(
            piece, piece, s_far.at[4 + block], r_far.at[y * 2 + x], worker(block, z)
        )

    def w_outer(kind, part):
        return remote(
            w_src(kind, part),
            w_slot(kind, z, part),
            s_w.at[w_sem(kind, 0, part)],
            r_w.at[w_sem(kind, 2, part)],
            (y, inner_z, twin),
        )

    def w_mid(kind, part):
        return remote(
            w_src(kind, part),
            w_slot(kind, z, part),
            s_w.at[w_sem(kind, 0, part)],
            r_w.at[w_sem(kind, 1, part)],
            (y, mid_z, t),
        )

    def w_relay(kind, part):
        piece = w_slot(kind, outer_z, part)
        return [
            remote(
                piece, piece, s_w.at[w_sem(kind, 0, part)], r_w.at[w_sem(kind, 3, part)],
                (y, mid_z, twin),
            ),
            remote(
                piece, piece, s_w.at[w_sem(kind, 1, part)], r_w.at[w_sem(kind, 2, part)],
                (y, z, twin),
            ),
        ]

    def start(copies):
        for copy in copies:
            copy.start()

    def sent(copies):
        for copy in copies:
            copy.wait_send()

    def part_send(rep, half, block, part):
        return remote(
            stage.at[rep, block, part, pl.ds(half * rows, rows), :],
            parts_in.at[t, part],
            s_out.at[((block * PARTS + part) * 2 + rep) * 2 + half],
            r_out.at[t * PARTS + part],
            (rep, base_z + half, block),
        )

    def to_other(rep, half, block):
        own = jnp.logical_and(jnp.logical_and(block == t, y == rep), z == base_z + half)
        return jnp.logical_not(own)

    def conv_sends():
        copies = []
        for a in range(2):
            for b in range(2):
                for d in range(4):
                    if a or b or d:
                        level = z if b == 0 else base_z + 1 - z % 2
                        copies.append(
                            remote(
                                conv_all.at[t],
                                conv_all.at[t],
                                s_conv.at[len(copies)],
                                r_conv.at[t],
                                ((y + a) % 2, level, ts[d]),
                            )
                        )
        return copies

    @pl.when(is_outer)
    def _():
        start(grad_outer())

        @pl.when(lead)
        def _():
            start([w_outer(0, p) for p in range(PARTS)])

        start(saved_home())

        @pl.when(lead)
        def _():
            start([w_outer(k, p) for k, p in order[PARTS:]])

    @pl.when(is_relay)
    def _():
        start(grad_edge())
        start(saved_edge())
        start([grad_own(b) for b in range(4)])
        start(saved_home())
        for i in range(2):
            arrived(og_all.at[y, 2 * x + i, edge_rows(z), :], l_edge.at[i])
        start([relay_edge(b) for b in range(4)])
        for i in range(2):
            arrived(og_all.at[y, 2 * x + i, block_rows(outer_z), :], l_far.at[i])
        start([relay_outer(b) for b in range(4)])
        for kind, part in order:
            arrived(w_slot(kind, outer_z, part), r_w.at[w_sem(kind, 2, part)])
            start(w_relay(kind, part))

    @pl.when(is_worker)
    def _():
        start(grad_edge())
        start(saved_edge())
        start([w_mid(k, p) for k, p in order[:PARTS]])
        pltpu.make_async_copy(og, og_all.at[y, t, block_rows(z), :], r_og.at[y * 4 + t]).start()
        for block in range(4):

            @pl.when(block != t)
            def _(block=block):
                grad_own(block).start()

        slot = block_rows(z)
        pltpu.make_async_copy(gl, gl_all.at[y, slot, :], r_gl.at[y * 3]).start()
        pltpu.make_async_copy(ul, ul_all.at[y, slot, :], r_ul.at[y * 3]).start()
        for kind, part in order:
            pltpu.make_async_copy(
                w_src(kind, part), w_slot(kind, z, part), r_w.at[w_sem(kind, 0, part)]
            ).start()
        start([w_mid(k, p) for k, p in order[PARTS:]])

        blank = pl.ds(pl.multiple_of((z - 1) * (EDGE + 2 * rows), EDGE), EDGE)
        for rep in range(2):
            for block in range(4):
                og_all[rep, block, blank, :] = jnp.zeros((EDGE, width), bf16)
            gl_all[rep, blank, :] = jnp.zeros((EDGE, hid), bf16)
            ul_all[rep, blank, :] = jnp.zeros((EDGE, hid), bf16)
        act[...] = jnp.zeros_like(act)
        conv_own[...] = jnp.zeros_like(conv_own)

        for rep in range(2):
            for block in range(4):
                arrived(og_all.at[rep, block, block_rows(z), :], r_og.at[rep * 4 + block])
            for i in range(2):
                two = pl.ds(2 * i, 2)
                arrived(og_all.at[rep, two, edge_rows(z), :], r_edge.at[rep * 2 + i])
                arrived(og_all.at[rep, two, block_rows(outer_z), :], r_far.at[rep * 2 + i])

        def level_of(role):
            near = jnp.where(role % 2 == 0, z, mid_z)
            far = jnp.where(role % 2 == 0, outer_z, 3 - outer_z)
            return jnp.where(role < 2, near, far)

        big = 2 * 128
        full, rest = hid // big, hid % big

        def act_step(role, carry):
            level = level_of(role)
            for part in range(PARTS):
                arrived(w_slot(0, level, part), r_w.at[w_sem(0, role, part)])

            def block_step(i, carry):
                rep = i // full
                cols = pl.ds(pl.multiple_of((i % full) * big, big), big)
                act[rep, :, cols] += rows_dot(og_all[rep, level], wd[level, cols, :])
                return carry

            lax.fori_loop(0, 2 * full, block_step, 0)
            if rest:
                cols = pl.ds(full * big, rest)

                def rest_step(rep, carry):
                    act[rep, :, cols] += rows_dot(og_all[rep, level], wd[level, cols, :])
                    return carry

                lax.fori_loop(0, 2, rest_step, 0)
            return carry

        lax.fori_loop(0, 4, act_step, 0)

        lane = 128

        def tile_step(rep, i):
            cols = pl.ds(pl.multiple_of(i * lane, lane), lane)
            taps = cw[:, pl.ds(pl.multiple_of(t * hid + i * lane, lane), lane)].astype(f32)
            own = gl_all[rep, :, cols].astype(f32)
            before = pltpu.roll(own, 1, 0)
            behind = pltpu.roll(own, n_rows - 1, 0)
            gate = taps[0:1] * before + taps[1:2] * own + taps[2:3] * behind
            gelu_value, gelu_slope = gelu_parts(gate)
            grad = act[rep, :, cols]
            up_all[rep, :, cols] = (grad * gelu_value).astype(bf16)
            gate_grad = grad * ul_all[rep, :, cols].astype(f32) * gelu_slope
            lin_all[rep, :, cols] = (
                taps[0:1] * pltpu.roll(gate_grad, n_rows - 1, 0)
                + taps[1:2] * gate_grad
                + taps[2:3] * pltpu.roll(gate_grad, 1, 0)
            ).astype(bf16)
            kept = slice(EDGE, EDGE + 2 * rows)
            for row, other in enumerate((before, own, behind)):
                conv_own[row : row + 1, cols] += jnp.sum(
                    gate_grad[kept] * other[kept], axis=0, keepdims=True
                )

        for turn in range(2):
            rep = 1 - y if turn == 0 else y
            for kind, slot in enumerate((block_rows(z), block_rows(outer_z), edge_rows(z))):
                arrived(gl_all.at[rep, slot, :], r_gl.at[rep * 3 + kind])
                arrived(ul_all.at[rep, slot, :], r_ul.at[rep * 3 + kind])

            def turn_step(i, carry, rep=rep):
                tile_step(rep, i)
                return carry

            lax.fori_loop(0, hid // lane, turn_step, 0)

        kept = pl.ds(EDGE, 2 * rows)
        step_cols = width // PARTS

        def emit(level, first, count):
            size = count * step_cols
            cols = pl.ds(pl.multiple_of(first * step_cols, step_cols), size)
            for rep in range(2):
                product = rows_dot(up_all[rep, kept, :], wu[level, cols, :]) + rows_dot(
                    lin_all[rep, kept, :], wg[level, cols, :]
                )
                product = product.astype(bf16)
                for k in range(count):
                    stage[rep, level, first + k] = product[:, k * step_cols : (k + 1) * step_cols]
            for rep in range(2):
                for half in range(2):
                    away = to_other(rep, half, level)

                    @pl.when(away)
                    def _(rep=rep, half=half):
                        for k in range(count):
                            part_send(rep, half, level, first + k).start()

                    @pl.when(jnp.logical_not(away))
                    def _(rep=rep, half=half):
                        for k in range(count):
                            parts_in[t, first + k] = stage[
                                rep, level, first + k, pl.ds(half * rows, rows), :
                            ]

        def wait_w(role, level, first, count):
            for k in range(count):
                for kind in (1, 2):
                    size = width // PARTS
                    slot = pl.ds(pl.multiple_of((first + k) * size, size), size)
                    buffer = (wg, wu)[kind - 1]
                    arrived(
                        buffer.at[level, slot, :], r_w.at[w_sem(kind, role, first + k)]
                    )

        def double_step(i, carry):
            role, first = i // 2, 2 * (i % 2)
            level = level_of(role)
            wait_w(role, level, first, 2)
            emit(level, first, 2)
            return carry

        lax.fori_loop(0, 2, double_step, 0)

        handed = remote(conv_own, conv_mid, s_mid.at[0], r_mid.at[0], (y, mid_z, t))
        handed.start()
        lax.fori_loop(2, 4, double_step, 0)
        arrived(conv_mid, r_mid.at[0])
        conv_all[t] = conv_own[...] + conv_mid[...]
        lax.fori_loop(4, 5, double_step, 0)
        start(conv_sends())
        lax.fori_loop(5, 6, double_step, 0)

        def single_step(part, carry):
            level = level_of(3)
            wait_w(3, level, part, 1)
            emit(level, part, 1)
            return carry

        lax.fori_loop(0, PARTS, single_step, 0)
        sent([handed])

    def remote_block(block):
        return jnp.logical_not(jnp.logical_and(is_worker, t == block))

    for block in range(4):

        @pl.when(remote_block(block))
        def _(block=block):
            arrived(conv_all.at[block], r_conv.at[block])

        cg[:, pl.ds(block * hid, hid)] = conv_all[block, 0:3, :]

    step_cols = width // PARTS
    for part in range(PARTS):
        for block in range(4):

            @pl.when(remote_block(block))
            def _(block=block):
                arrived(parts_in.at[block, part], r_out.at[block * PARTS + part])

        total = parts_in[0, part].astype(f32)
        for block in range(1, 4):
            total = total + parts_in[block, part].astype(f32)
        out[:, part * step_cols : (part + 1) * step_cols] = total.astype(out.dtype)

    @pl.when(is_outer)
    def _():
        sent(grad_outer())
        sent(saved_home())

        @pl.when(lead)
        def _():
            sent([w_outer(k, p) for k, p in order])

    @pl.when(is_relay)
    def _():
        sent(grad_edge())
        sent(saved_edge())
        sent([grad_own(b) for b in range(4)])
        sent(saved_home())
        sent([relay_edge(b) for b in range(4)])
        sent([relay_outer(b) for b in range(4)])
        for kind, part in order:
            sent(w_relay(kind, part))

    @pl.when(is_worker)
    def _():
        sent(grad_edge())
        sent(saved_edge())
        sent([w_mid(k, p) for k, p in order])
        for block in range(4):

            @pl.when(block != t)
            def _(block=block):
                grad_own(block).wait_send()

        sent(conv_sends())

        def done_step(i, carry):
            block, part = i // PARTS, i % PARTS
            for rep in range(2):
                for half in range(2):

                    @pl.when(to_other(rep, half, block))
                    def _(rep=rep, half=half):
                        part_send(rep, half, block, part).wait_send()

            return carry

        lax.fori_loop(0, 4 * PARTS, done_step, 0)


def fused(out_grad, gate_lin, up_lin, conv_weight, gate_weight, up_weight, down_weight):
    f32, bf16 = jnp.float32, jnp.bfloat16
    rows, width = out_grad.shape
    hid = gate_lin.shape[1]
    n_rows = 2 * rows + 2 * EDGE
    dma = pltpu.SemaphoreType.DMA
    hbm = pl.BlockSpec(memory_space=pl.ANY)
    vmem = pl.BlockSpec(memory_space=pltpu.VMEM)
    return pl.pallas_call(
        kernel,
        out_shape=(
            jax.ShapeDtypeStruct((rows, width), bf16),
            jax.ShapeDtypeStruct((3, 4 * hid), f32),
        ),
        in_specs=[hbm, hbm, hbm, vmem, hbm, hbm, hbm],
        out_specs=(vmem, vmem),
        scratch_shapes=[
            pltpu.VMEM((2, 4, n_rows, width), bf16),
            pltpu.VMEM((2, n_rows, hid), bf16),
            pltpu.VMEM((2, n_rows, hid), bf16),
            pltpu.VMEM((2, n_rows, hid), f32),
            pltpu.VMEM((2, n_rows, hid), bf16),
            pltpu.VMEM((2, n_rows, hid), bf16),
            pltpu.VMEM((4, hid, width), bf16),
            pltpu.VMEM((4, width, hid), bf16),
            pltpu.VMEM((4, width, hid), bf16),
            pltpu.VMEM((2, 4, PARTS, 2 * rows, width // PARTS), bf16),
            pltpu.VMEM((4, PARTS, rows, width // PARTS), bf16),
            pltpu.VMEM((8, hid), f32),
            pltpu.VMEM((8, hid), f32),
            pltpu.VMEM((4, 8, hid), f32),
        ]
        + [dma((n,)) for n in (8, 4, 4, 2, 2, 6, 6, 12 * PARTS, 4 * PARTS, 1, 4)]
        + [dma((n,)) for n in (4, 8, 1, 2, 2, 1, 12 * PARTS, 16 * PARTS, 1, 15)],
        compiler_params=pltpu.CompilerParams(
            collective_id=0, has_side_effects=True, vmem_limit_bytes=67_000_000
        ),
    )(out_grad, gate_lin, up_lin, conv_weight, gate_weight, up_weight, down_weight)


def solution(mesh):
    sizes = tuple(mesh.shape[a] for a in ("rep", "fs", "tp"))
    return jax.shard_map(
        fused if sizes == (2, 4, 4) else local,
        mesh=mesh,
        in_specs=(
            P(("rep", "fs"), "tp"),
            P(("rep", "fs"), "tp"),
            P(("rep", "fs"), "tp"),
            P(),
            P("fs", "tp"),
            P("fs", "tp"),
            P("tp", "fs"),
        ),
        out_specs=(P(("rep", "fs"), "tp"), P()),
        check_vma=False,
    )
```

profile of v0, /device:TPU:3, one launch (start us, length us, event | category | flops | bytes accessed | tf_op | source)
XLA Modules:
  0.0 126.6 jit_solution(4674492080158432038)
XLA Ops:
  0.6 122.7 %shard_map.86 = (bf16[256,512]{1,0:T(8,128)(2,1)}, f32[3,5632]{1,0:T(4,128)}) custom-call(bf16[256,512]{1,0:T(8,128)(2,1)} %og.1, bf16[256,1408]{1,0:T(8,128)(2,1)} %gl.1, bf16[256,1408]{1,0:T(8,128)(2,1)} %ul.1, bf16[3,5632]{1,0:T(4,128)(2,1)} %cw.1, bf16[512,1408]{1,0:T(8,128)(2,1)} %gw.1, bf16[512,1408]{1,0:T(8,128)(2,1)} %uw.1, bf16[1408,512]{1,0:T(8,128)(2,1)} %dw.1), custom_call_target="tpu_custom_call" | custom-call | tf_op jit(solution)/shard_map/pallas_call | solution.py:603
  123.3 1.7 %copy.11 = bf16[256,512]{1,0:T(8,128)(2,1)} copy(bf16[256,512]{1,0:T(8,128)(2,1)} %get-tuple-element.4) | data formatting | bytes 524288
  125.0 1.5 %copy.12 = f32[3,5632]{1,0:T(4,128)} copy(f32[3,5632]{1,0:T(4,128)} %get-tuple-element.5) | data formatting | bytes 135168
where the time goes:
time: 127 us
  Pallas kernels  123 us (97%)
  local copies, waits for them, and re-layouts  3.21 us (3%)
    pallas_call x1, Pallas kernels, fused(): pl.pallas_call(kernel, out_shape=(jax.ShapeDtypeStruct((rows, width), bf1...  123 us
    unnamed x2, local copies, waits for them, and re-layouts  3.21 us

commit v1 on v0

--- a/solution.py
+++ b/solution.py
@@ -107,7 +107,7 @@
     og, gl, ul, cw, gw, uw, dw, out, cg,
     og_all, gl_all, ul_all, act, up_all, lin_all, wd, wg, wu,
     stage, parts_in, conv_own, conv_mid, conv_all,
-    r_og, r_far, r_edge, l_far, l_edge, r_gl, r_ul, r_w, r_out, r_mid, r_conv,
+    r_og, r_far, r_edge, l_far, l_edge, l_saved, r_gl, r_ul, r_w, r_out, r_mid, r_conv,
     s_og, s_far, s_edge, s_gl, s_ul, s_hand, s_w, s_out, s_mid, s_conv,
 ):
     f32, bf16 = jnp.float32, jnp.bfloat16
@@ -129,11 +129,12 @@
     is_relay = jnp.logical_and(inner, core != y)
     is_outer = z != inner_z
 
-    def block_rows(level):
-        return pl.ds(pl.multiple_of(EDGE + (level % 2) * rows, EDGE), rows)
-
-    def edge_rows(level):
-        return pl.ds(pl.multiple_of((2 - level) * (EDGE + 2 * rows), EDGE), EDGE)
+    def block_rows(rep, level):
+        return pl.ds(pl.multiple_of(rep * n_rows + EDGE + (level % 2) * rows, EDGE), rows)
+
+    def edge_rows(rep, level):
+        start = rep * n_rows + (2 - level) * (EDGE + 2 * rows)
+        return pl.ds(pl.multiple_of(start, EDGE), EDGE)
 
     edge_src = pl.ds(pl.multiple_of((2 - inner_z) * (rows - EDGE), EDGE), EDGE)
 
@@ -188,29 +189,42 @@
     def saved_home():
         goal = worker(t, inner_z)
         kind = jnp.where(inner, 0, 1)
-        slot = block_rows(z)
+        slot = block_rows(y, z)
         return [
-            remote(gl, gl_all.at[y, slot, :], s_gl.at[0], r_gl.at[y * 3 + kind], goal),
-            remote(ul, ul_all.at[y, slot, :], s_ul.at[0], r_ul.at[y * 3 + kind], goal),
+            remote(gl, gl_all.at[slot, :], s_gl.at[0], r_gl.at[y * 3 + kind], goal),
+            remote(ul, ul_all.at[slot, :], s_ul.at[0], r_ul.at[y * 3 + kind], goal),
+        ]
+
+    def saved_across():
+        goal = (1 - y, z, t)
+        slot = block_rows(y, z)
+        return [
+            remote(gl, gl_all.at[slot, :], s_gl.at[0], l_saved.at[0], goal),
+            remote(ul, ul_all.at[slot, :], s_ul.at[0], l_saved.at[1], goal),
+        ]
+
+    def saved_onward():
+        goal = (y, inner_z, t)
+        gl_piece, ul_piece = (ref.at[block_rows(1 - y, z), :] for ref in (gl_all, ul_all))
+        kind = (1 - y) * 3 + 1
+        return [
+            remote(gl_piece, gl_piece, s_gl.at[1], r_gl.at[kind], goal),
+            remote(ul_piece, ul_piece, s_ul.at[1], r_ul.at[kind], goal),
         ]
 
     def saved_edge():
         goal = worker(t, mid_z)
-        slot = edge_rows(mid_z)
+        slot = edge_rows(y, mid_z)
         return [
-            remote(
-                gl.at[edge_src, :], gl_all.at[y, slot, :], s_gl.at[1], r_gl.at[y * 3 + 2], goal
-            ),
-            remote(
-                ul.at[edge_src, :], ul_all.at[y, slot, :], s_ul.at[1], r_ul.at[y * 3 + 2], goal
-            ),
+            remote(gl.at[edge_src, :], gl_all.at[slot, :], s_gl.at[1], r_gl.at[y * 3 + 2], goal),
+            remote(ul.at[edge_src, :], ul_all.at[slot, :], s_ul.at[1], r_ul.at[y * 3 + 2], goal),
         ]
 
     def grad_edge():
         return [
             remote(
                 og.at[edge_src, :],
-                og_all.at[y, t, edge_rows(mid_z), :],
+                og_all.at[t, edge_rows(y, mid_z), :],
                 s_edge.at[0],
                 l_edge.at[core],
                 (y, mid_z, relay_t),
@@ -219,7 +233,7 @@
 
     def grad_own(block):
         return remote(
-            og, og_all.at[y, t, block_rows(z), :], s_og.at[block], r_og.at[y * 4 + t],
+            og, og_all.at[t, block_rows(y, z), :], s_og.at[block], r_og.at[y * 4 + t],
             worker(block, z),
         )
 
@@ -227,7 +241,7 @@
         return [
             remote(
                 og,
-                og_all.at[y, t, block_rows(z), :],
+                og_all.at[t, block_rows(y, z), :],
                 s_hand.at[0],
                 l_far.at[core],
                 (y, inner_z, relay_t),
@@ -235,16 +249,16 @@
         ]
 
     def pair(slot):
-        return og_all.at[y, pl.ds(2 * x, 2), slot, :]
+        return og_all.at[pl.ds(2 * x, 2), slot, :]
 
     def relay_edge(block):
-        piece = pair(edge_rows(z))
+        piece = pair(edge_rows(y, z))
         return remote(
             piece, piece, s_far.at[block], r_edge.at[y * 2 + x], worker(block, z)
         )
 
     def relay_outer(block):
-        piece = pair(block_rows(outer_z))
+        piece = pair(block_rows(y, outer_z))
         return remote(
             piece, piece, s_far.at[4 + block], r_far.at[y * 2 + x], worker(block, z)
         )
@@ -325,26 +339,29 @@
 
         @pl.when(lead)
         def _():
-            start([w_outer(0, p) for p in range(PARTS)])
-
-        start(saved_home())
-
-        @pl.when(lead)
+            start([w_outer(k, p) for k, p in order[:PARTS]])
+            for i, (copy, ref) in enumerate(zip(saved_onward(), (gl_all, ul_all))):
+                arrived(ref.at[block_rows(1 - y, z), :], l_saved.at[i])
+                copy.start()
+            start(saved_home())
+            start([w_outer(k, p) for k, p in order[PARTS:]])
+
+        @pl.when(core != y)
         def _():
-            start([w_outer(k, p) for k, p in order[PARTS:]])
+            start(saved_across())
 
     @pl.when(is_relay)
     def _():
         start(grad_edge())
         start(saved_edge())
         start([grad_own(b) for b in range(4)])
-        start(saved_home())
         for i in range(2):
-            arrived(og_all.at[y, 2 * x + i, edge_rows(z), :], l_edge.at[i])
+            arrived(og_all.at[2 * x + i, edge_rows(y, z), :], l_edge.at[i])
         start([relay_edge(b) for b in range(4)])
         for i in range(2):
-            arrived(og_all.at[y, 2 * x + i, block_rows(outer_z), :], l_far.at[i])
+            arrived(og_all.at[2 * x + i, block_rows(y, outer_z), :], l_far.at[i])
         start([relay_outer(b) for b in range(4)])
+        start(saved_home())
         for kind, part in order:
             arrived(w_slot(kind, outer_z, part), r_w.at[w_sem(kind, 2, part)])
             start(w_relay(kind, part))
@@ -354,38 +371,38 @@
         start(grad_edge())
         start(saved_edge())
         start([w_mid(k, p) for k, p in order[:PARTS]])
-        pltpu.make_async_copy(og, og_all.at[y, t, block_rows(z), :], r_og.at[y * 4 + t]).start()
+        pltpu.make_async_copy(og, og_all.at[t, block_rows(y, z), :], r_og.at[y * 4 + t]).start()
         for block in range(4):
 
             @pl.when(block != t)
             def _(block=block):
                 grad_own(block).start()
 
-        slot = block_rows(z)
-        pltpu.make_async_copy(gl, gl_all.at[y, slot, :], r_gl.at[y * 3]).start()
-        pltpu.make_async_copy(ul, ul_all.at[y, slot, :], r_ul.at[y * 3]).start()
+        slot = block_rows(y, z)
+        pltpu.make_async_copy(gl, gl_all.at[slot, :], r_gl.at[y * 3]).start()
+        pltpu.make_async_copy(ul, ul_all.at[slot, :], r_ul.at[y * 3]).start()
         for kind, part in order:
             pltpu.make_async_copy(
                 w_src(kind, part), w_slot(kind, z, part), r_w.at[w_sem(kind, 0, part)]
             ).start()
-        start([w_mid(k, p) for k, p in order[PARTS:]])
-
-        blank = pl.ds(pl.multiple_of((z - 1) * (EDGE + 2 * rows), EDGE), EDGE)
+
+        for rep in range(2):
+            first = rep * n_rows + (z - 1) * (EDGE + 2 * rows)
+            blank = pl.ds(pl.multiple_of(first, EDGE), EDGE)
+            for block in range(4):
+                og_all[block, blank, :] = jnp.zeros((EDGE, width), bf16)
+            gl_all[blank, :] = jnp.zeros((EDGE, hid), bf16)
+            ul_all[blank, :] = jnp.zeros((EDGE, hid), bf16)
+        act[...] = jnp.zeros_like(act)
+        conv_own[...] = jnp.zeros_like(conv_own)
+
         for rep in range(2):
             for block in range(4):
-                og_all[rep, block, blank, :] = jnp.zeros((EDGE, width), bf16)
-            gl_all[rep, blank, :] = jnp.zeros((EDGE, hid), bf16)
-            ul_all[rep, blank, :] = jnp.zeros((EDGE, hid), bf16)
-        act[...] = jnp.zeros_like(act)
-        conv_own[...] = jnp.zeros_like(conv_own)
-
-        for rep in range(2):
-            for block in range(4):
-                arrived(og_all.at[rep, block, block_rows(z), :], r_og.at[rep * 4 + block])
+                arrived(og_all.at[block, block_rows(rep, z), :], r_og.at[rep * 4 + block])
             for i in range(2):
                 two = pl.ds(2 * i, 2)
-                arrived(og_all.at[rep, two, edge_rows(z), :], r_edge.at[rep * 2 + i])
-                arrived(og_all.at[rep, two, block_rows(outer_z), :], r_far.at[rep * 2 + i])
+                arrived(og_all.at[two, edge_rows(rep, z), :], r_edge.at[rep * 2 + i])
+                arrived(og_all.at[two, block_rows(rep, outer_z), :], r_far.at[rep * 2 + i])
 
         def level_of(role):
             near = jnp.where(role % 2 == 0, z, mid_z)
@@ -395,44 +412,48 @@
         big = 2 * 128
         full, rest = hid // big, hid % big
 
+        def act_product(level):
+            def block_step(i, carry):
+                cols = pl.ds(pl.multiple_of(i * big, big), big)
+                act[:, cols] += rows_dot(og_all[level], wd[level, cols, :])
+                return carry
+
+            lax.fori_loop(0, full, block_step, 0)
+            if rest:
+                cols = pl.ds(full * big, rest)
+                act[:, cols] += rows_dot(og_all[level], wd[level, cols, :])
+
         def act_step(role, carry):
             level = level_of(role)
             for part in range(PARTS):
                 arrived(w_slot(0, level, part), r_w.at[w_sem(0, role, part)])
-
-            def block_step(i, carry):
-                rep = i // full
-                cols = pl.ds(pl.multiple_of((i % full) * big, big), big)
-                act[rep, :, cols] += rows_dot(og_all[rep, level], wd[level, cols, :])
-                return carry
-
-            lax.fori_loop(0, 2 * full, block_step, 0)
-            if rest:
-                cols = pl.ds(full * big, rest)
-
-                def rest_step(rep, carry):
-                    act[rep, :, cols] += rows_dot(og_all[rep, level], wd[level, cols, :])
-                    return carry
-
-                lax.fori_loop(0, 2, rest_step, 0)
+            act_product(level)
             return carry
 
-        lax.fori_loop(0, 4, act_step, 0)
+        lax.fori_loop(0, 2, act_step, 0)
+        arrived(w_slot(0, 3 - outer_z, PARTS - 2), r_w.at[w_sem(0, 3, PARTS - 2)])
+        start([w_mid(k, p) for k, p in order[PARTS:]])
+        act_step(2, 0)
+        for part in range(PARTS):
+            if part != PARTS - 2:
+                arrived(w_slot(0, 3 - outer_z, part), r_w.at[w_sem(0, 3, part)])
+        act_product(3 - outer_z)
 
         lane = 128
 
         def tile_step(rep, i):
+            span = pl.ds(pl.multiple_of(rep * n_rows, EDGE), n_rows)
             cols = pl.ds(pl.multiple_of(i * lane, lane), lane)
             taps = cw[:, pl.ds(pl.multiple_of(t * hid + i * lane, lane), lane)].astype(f32)
-            own = gl_all[rep, :, cols].astype(f32)
+            own = gl_all[span, cols].astype(f32)
             before = pltpu.roll(own, 1, 0)
             behind = pltpu.roll(own, n_rows - 1, 0)
             gate = taps[0:1] * before + taps[1:2] * own + taps[2:3] * behind
             gelu_value, gelu_slope = gelu_parts(gate)
-            grad = act[rep, :, cols]
-            up_all[rep, :, cols] = (grad * gelu_value).astype(bf16)
-            gate_grad = grad * ul_all[rep, :, cols].astype(f32) * gelu_slope
-            lin_all[rep, :, cols] = (
+            grad = act[span, cols]
+            up_all[span, cols] = (grad * gelu_value).astype(bf16)
+            gate_grad = grad * ul_all[span, cols].astype(f32) * gelu_slope
+            lin_all[span, cols] = (
                 taps[0:1] * pltpu.roll(gate_grad, n_rows - 1, 0)
                 + taps[1:2] * gate_grad
                 + taps[2:3] * pltpu.roll(gate_grad, 1, 0)
@@ -445,9 +466,10 @@
 
         for turn in range(2):
             rep = 1 - y if turn == 0 else y
-            for kind, slot in enumerate((block_rows(z), block_rows(outer_z), edge_rows(z))):
-                arrived(gl_all.at[rep, slot, :], r_gl.at[rep * 3 + kind])
-                arrived(ul_all.at[rep, slot, :], r_ul.at[rep * 3 + kind])
+            slots = (block_rows(rep, z), block_rows(rep, outer_z), edge_rows(rep, z))
+            for kind, slot in enumerate(slots):
+                arrived(gl_all.at[slot, :], r_gl.at[rep * 3 + kind])
+                arrived(ul_all.at[slot, :], r_ul.at[rep * 3 + kind])
 
             def turn_step(i, carry, rep=rep):
                 tile_step(rep, i)
@@ -455,19 +477,21 @@
 
             lax.fori_loop(0, hid // lane, turn_step, 0)
 
-        kept = pl.ds(EDGE, 2 * rows)
         step_cols = width // PARTS
 
-        def emit(level, first, count):
+        def product(side, weight, level, first, count):
             size = count * step_cols
             cols = pl.ds(pl.multiple_of(first * step_cols, step_cols), size)
+            return rows_dot(side[...], weight[level, cols, :])
+
+        def emit(total, level, first, count):
+            total = total.astype(bf16)
             for rep in range(2):
-                product = rows_dot(up_all[rep, kept, :], wu[level, cols, :]) + rows_dot(
-                    lin_all[rep, kept, :], wg[level, cols, :]
-                )
-                product = product.astype(bf16)
+                kept = slice(rep * n_rows + EDGE, rep * n_rows + EDGE + 2 * rows)
                 for k in range(count):
-                    stage[rep, level, first + k] = product[:, k * step_cols : (k + 1) * step_cols]
+                    stage[rep, level, first + k] = total[
+                        kept, k * step_cols : (k + 1) * step_cols
+                    ]
             for rep in range(2):
                 for half in range(2):
                     away = to_other(rep, half, level)
@@ -484,21 +508,19 @@
                                 rep, level, first + k, pl.ds(half * rows, rows), :
                             ]
 
-        def wait_w(role, level, first, count):
-            for k in range(count):
-                for kind in (1, 2):
-                    size = width // PARTS
-                    slot = pl.ds(pl.multiple_of((first + k) * size, size), size)
-                    buffer = (wg, wu)[kind - 1]
-                    arrived(
-                        buffer.at[level, slot, :], r_w.at[w_sem(kind, role, first + k)]
-                    )
+        def wait_w(kind, role, level, part):
+            slot = pl.ds(pl.multiple_of(part * step_cols, step_cols), step_cols)
+            buffer = (wg, wu)[kind - 1]
+            arrived(buffer.at[level, slot, :], r_w.at[w_sem(kind, role, part)])
 
         def double_step(i, carry):
             role, first = i // 2, 2 * (i % 2)
             level = level_of(role)
-            wait_w(role, level, first, 2)
-            emit(level, first, 2)
+            for k in range(2):
+                for kind in (1, 2):
+                    wait_w(kind, role, level, first + k)
+            total = product(lin_all, wg, level, first, 2) + product(up_all, wu, level, first, 2)
+            emit(total, level, first, 2)
             return carry
 
         lax.fori_loop(0, 2, double_step, 0)
@@ -514,8 +536,10 @@
 
         def single_step(part, carry):
             level = level_of(3)
-            wait_w(3, level, part, 1)
-            emit(level, part, 1)
+            wait_w(1, 3, level, part)
+            total = product(lin_all, wg, level, part, 1)
+            wait_w(2, 3, level, part)
+            emit(total + product(up_all, wu, level, part, 1), level, part, 1)
             return carry
 
         lax.fori_loop(0, PARTS, single_step, 0)
@@ -548,11 +572,16 @@
     @pl.when(is_outer)
     def _():
         sent(grad_outer())
-        sent(saved_home())
 
         @pl.when(lead)
         def _():
             sent([w_outer(k, p) for k, p in order])
+            sent(saved_onward())
+            sent(saved_home())
+
+        @pl.when(core != y)
+        def _():
+            sent(saved_across())
 
     @pl.when(is_relay)
     def _():
@@ -609,12 +638,12 @@
         in_specs=[hbm, hbm, hbm, vmem, hbm, hbm, hbm],
         out_specs=(vmem, vmem),
         scratch_shapes=[
-            pltpu.VMEM((2, 4, n_rows, width), bf16),
-            pltpu.VMEM((2, n_rows, hid), bf16),
-            pltpu.VMEM((2, n_rows, hid), bf16),
-            pltpu.VMEM((2, n_rows, hid), f32),
-            pltpu.VMEM((2, n_rows, hid), bf16),
-            pltpu.VMEM((2, n_rows, hid), bf16),
+            pltpu.VMEM((4, 2 * n_rows, width), bf16),
+            pltpu.VMEM((2 * n_rows, hid), bf16),
+            pltpu.VMEM((2 * n_rows, hid), bf16),
+            pltpu.VMEM((2 * n_rows, hid), f32),
+            pltpu.VMEM((2 * n_rows, hid), bf16),
+            pltpu.VMEM((2 * n_rows, hid), bf16),
             pltpu.VMEM((4, hid, width), bf16),
             pltpu.VMEM((4, width, hid), bf16),
             pltpu.VMEM((4, width, hid), bf16),
@@ -624,7 +653,7 @@
             pltpu.VMEM((8, hid), f32),
             pltpu.VMEM((4, 8, hid), f32),
         ]
-        + [dma((n,)) for n in (8, 4, 4, 2, 2, 6, 6, 12 * PARTS, 4 * PARTS, 1, 4)]
+        + [dma((n,)) for n in (8, 4, 4, 2, 2, 2, 6, 6, 12 * PARTS, 4 * PARTS, 1, 4)]
         + [dma((n,)) for n in (4, 8, 1, 2, 2, 1, 12 * PARTS, 16 * PARTS, 1, 15)],
         compiler_params=pltpu.CompilerParams(
             collective_id=0, has_side_effects=True, vmem_limit_bytes=67_000_000

time: 127 us -> 116 us (0.913)
  Pallas kernels: 123 us -> 111 us
    pallas_call x1, Pallas kernels: 123 us -> 111 us  [fused(): pl.pallas_call(kernel, out_shape=(jax.ShapeDtypeStruct((rows, width), bf1...]
where the time goes in v1:
time: 116 us; the launch traced here: 115 us
  Pallas kernels  111 us (96%)
  local copies, waits for them, and re-layouts  3.21 us (3%)
    pallas_call x1, Pallas kernels, fused(): pl.pallas_call(kernel, out_shape=(jax.ShapeDtypeStruct((rows, width), bf1...  111 us
    unnamed x2, local copies, waits for them, and re-layouts  3.21 us

profile of v1, /device:TPU:3, one launch (start us, length us, event | category | flops | bytes accessed | tf_op | source)
XLA Modules:
  0.0 114.9 jit_solution(17869180904036435249)
XLA Ops:
  0.6 111.1 %shard_map.86 = (bf16[256,512]{1,0:T(8,128)(2,1)}, f32[3,5632]{1,0:T(4,128)}) custom-call(bf16[256,512]{1,0:T(8,128)(2,1)} %og.1, bf16[256,1408]{1,0:T(8,128)(2,1)} %gl.1, bf16[256,1408]{1,0:T(8,128)(2,1)} %ul.1, bf16[3,5632]{1,0:T(4,128)(2,1)} %cw.1, bf16[512,1408]{1,0:T(8,128)(2,1)} %gw.1, bf16[512,1408]{1,0:T(8,128)(2,1)} %uw.1, bf16[1408,512]{1,0:T(8,128)(2,1)} %dw.1), custom_call_target="tpu_custom_call" | custom-call | tf_op jit(solution)/shard_map/pallas_call | solution.py:632
  111.7 1.7 %copy.11 = bf16[256,512]{1,0:T(8,128)(2,1)} copy(bf16[256,512]{1,0:T(8,128)(2,1)} %get-tuple-element.4) | data formatting | bytes 524288
  113.4 1.5 %copy.12 = f32[3,5632]{1,0:T(4,128)} copy(f32[3,5632]{1,0:T(4,128)} %get-tuple-element.5) | data formatting | bytes 135168

commit v2 on v1

--- a/solution.py
+++ b/solution.py
@@ -106,9 +106,9 @@
 def kernel(
     og, gl, ul, cw, gw, uw, dw, out, cg,
     og_all, gl_all, ul_all, act, up_all, lin_all, wd, wg, wu,
-    stage, parts_in, conv_own, conv_mid, conv_all,
-    r_og, r_far, r_edge, l_far, l_edge, l_saved, r_gl, r_ul, r_w, r_out, r_mid, r_conv,
-    s_og, s_far, s_edge, s_gl, s_ul, s_hand, s_w, s_out, s_mid, s_conv,
+    stage, parts_in, taps_own, conv_own, conv_mid, conv_all,
+    r_og, l_far, l_edge, l_saved, l_taps, r_saved, r_w, r_out, r_mid, r_conv,
+    s_og, s_far, s_edge, s_saved, s_w, s_out, s_mid, s_conv,
 ):
     f32, bf16 = jnp.float32, jnp.bfloat16
     y, z, t = (lax.axis_index(a) for a in ("rep", "fs", "tp"))
@@ -183,41 +183,43 @@
 
     order = [(0, p) for p in range(PARTS)] + [(k, p) for p in range(PARTS) for k in (1, 2)]
 
-    def w_sem(kind, role, part):
-        return (kind * 4 + role) * PARTS + part
+    landing = {piece: i for i, piece in enumerate(order)}
+    last = (2, PARTS - 1)
+    cut = (hid // 128 + 1) // 2 * 128
+
+    DOWN_OWN, DOWN_NEAR, DOWN_OUTER, DOWN_FAR, DOWN_LAST, BOTH_OWN, BOTH_NEAR, BOTH_OUTER = range(8)
+    BOTH_FAR = BOTH_OUTER + 2
 
     def saved_home():
         goal = worker(t, inner_z)
-        kind = jnp.where(inner, 0, 1)
         slot = block_rows(y, z)
         return [
-            remote(gl, gl_all.at[slot, :], s_gl.at[0], r_gl.at[y * 3 + kind], goal),
-            remote(ul, ul_all.at[slot, :], s_ul.at[0], r_ul.at[y * 3 + kind], goal),
+            remote(gl, gl_all.at[slot, :], s_saved.at[0], r_saved.at[y], goal),
+            remote(ul, ul_all.at[slot, :], s_saved.at[0], r_saved.at[y], goal),
         ]
 
     def saved_across():
         goal = (1 - y, z, t)
         slot = block_rows(y, z)
         return [
-            remote(gl, gl_all.at[slot, :], s_gl.at[0], l_saved.at[0], goal),
-            remote(ul, ul_all.at[slot, :], s_ul.at[0], l_saved.at[1], goal),
+            remote(gl, gl_all.at[slot, :], s_saved.at[0], l_saved.at[0], goal),
+            remote(ul, ul_all.at[slot, :], s_saved.at[0], l_saved.at[1], goal),
         ]
 
     def saved_onward():
         goal = (y, inner_z, t)
         gl_piece, ul_piece = (ref.at[block_rows(1 - y, z), :] for ref in (gl_all, ul_all))
-        kind = (1 - y) * 3 + 1
         return [
-            remote(gl_piece, gl_piece, s_gl.at[1], r_gl.at[kind], goal),
-            remote(ul_piece, ul_piece, s_ul.at[1], r_ul.at[kind], goal),
+            remote(gl_piece, gl_piece, s_saved.at[0], r_saved.at[1 - y], goal),
+            remote(ul_piece, ul_piece, s_saved.at[0], r_saved.at[1 - y], goal),
         ]
 
     def saved_edge():
         goal = worker(t, mid_z)
         slot = edge_rows(y, mid_z)
         return [
-            remote(gl.at[edge_src, :], gl_all.at[slot, :], s_gl.at[1], r_gl.at[y * 3 + 2], goal),
-            remote(ul.at[edge_src, :], ul_all.at[slot, :], s_ul.at[1], r_ul.at[y * 3 + 2], goal),
+            remote(gl.at[edge_src, :], gl_all.at[slot, :], s_saved.at[0], r_saved.at[y], goal),
+            remote(ul.at[edge_src, :], ul_all.at[slot, :], s_saved.at[0], r_saved.at[y], goal),
         ]
 
     def grad_edge():
@@ -226,14 +228,14 @@
                 og.at[edge_src, :],
                 og_all.at[t, edge_rows(y, mid_z), :],
                 s_edge.at[0],
-                l_edge.at[core],
+                l_edge.at[0],
                 (y, mid_z, relay_t),
             )
         ]
 
     def grad_own(block):
         return remote(
-            og, og_all.at[t, block_rows(y, z), :], s_og.at[block], r_og.at[y * 4 + t],
+            og, og_all.at[t, block_rows(y, z), :], s_og.at[0], r_og.at[0],
             worker(block, z),
         )
 
@@ -242,8 +244,8 @@
             remote(
                 og,
                 og_all.at[t, block_rows(y, z), :],
-                s_hand.at[0],
-                l_far.at[core],
+                s_edge.at[0],
+                l_far.at[0],
                 (y, inner_z, relay_t),
             )
         ]
@@ -254,60 +256,63 @@
     def relay_edge(block):
         piece = pair(edge_rows(y, z))
         return remote(
-            piece, piece, s_far.at[block], r_edge.at[y * 2 + x], worker(block, z)
+            piece, piece, s_far.at[0], r_og.at[0], worker(block, z)
         )
 
     def relay_outer(block):
         piece = pair(block_rows(y, outer_z))
         return remote(
-            piece, piece, s_far.at[4 + block], r_far.at[y * 2 + x], worker(block, z)
+            piece, piece, s_far.at[0], r_og.at[0], worker(block, z)
         )
 
     def w_outer(kind, part):
         return remote(
             w_src(kind, part),
             w_slot(kind, z, part),
-            s_w.at[w_sem(kind, 0, part)],
-            r_w.at[w_sem(kind, 2, part)],
+            s_w.at[0],
+            r_w.at[landing[kind, part]],
             (y, inner_z, twin),
         )
 
     def w_mid(kind, part):
+        sem = DOWN_NEAR if kind == 0 else BOTH_NEAR
         return remote(
-            w_src(kind, part),
-            w_slot(kind, z, part),
-            s_w.at[w_sem(kind, 0, part)],
-            r_w.at[w_sem(kind, 1, part)],
-            (y, mid_z, t),
+            w_src(kind, part), w_slot(kind, z, part), s_w.at[0], r_w.at[sem], (y, mid_z, t)
         )
+
+    def far_sem(kind, part):
+        if kind == 0:
+            return DOWN_LAST if part == PARTS - 1 else DOWN_FAR
+        return BOTH_FAR + 2 * part + kind - 1
 
     def w_relay(kind, part):
         piece = w_slot(kind, outer_z, part)
-        return [
-            remote(
-                piece, piece, s_w.at[w_sem(kind, 0, part)], r_w.at[w_sem(kind, 3, part)],
-                (y, mid_z, twin),
-            ),
-            remote(
-                piece, piece, s_w.at[w_sem(kind, 1, part)], r_w.at[w_sem(kind, 2, part)],
-                (y, z, twin),
-            ),
-        ]
+        goal = (y, mid_z, twin)
+        sem = far_sem(kind, part)
+        if (kind, part) == last:
+            ends = (piece.at[:, pl.ds(0, cut)], piece.at[:, pl.ds(cut, hid - cut)])
+        else:
+            ends = (piece,)
+        copies = [remote(e, e, s_w.at[0], r_w.at[sem + i], goal) for i, e in enumerate(ends)]
+        sem = DOWN_OUTER if kind == 0 else BOTH_OUTER + part * 2 // PARTS
+        return copies + [remote(piece, piece, s_w.at[1], r_w.at[sem], (y, z, twin))]
 
     def start(copies):
         for copy in copies:
             copy.start()
 
-    def sent(copies):
-        for copy in copies:
-            copy.wait_send()
+    def og_bytes(count):
+        return og_all.at[:, pl.ds(0, count // 4), :]
+
+    def saved_bytes(count):
+        return gl_all.at[pl.ds(0, count), :]
 
     def part_send(rep, half, block, part):
         return remote(
             stage.at[rep, block, part, pl.ds(half * rows, rows), :],
             parts_in.at[t, part],
-            s_out.at[((block * PARTS + part) * 2 + rep) * 2 + half],
-            r_out.at[t * PARTS + part],
+            s_out.at[0],
+            r_out.at[part // (PARTS - 1)],
             (rep, base_z + half, block),
         )
 
@@ -326,8 +331,8 @@
                             remote(
                                 conv_all.at[t],
                                 conv_all.at[t],
-                                s_conv.at[len(copies)],
-                                r_conv.at[t],
+                                s_conv.at[0],
+                                r_conv.at[0],
                                 ((y + a) % 2, level, ts[d]),
                             )
                         )
@@ -355,23 +360,22 @@
         start(grad_edge())
         start(saved_edge())
         start([grad_own(b) for b in range(4)])
-        for i in range(2):
-            arrived(og_all.at[2 * x + i, edge_rows(y, z), :], l_edge.at[i])
+        arrived(pair(edge_rows(y, z)), l_edge.at[0])
         start([relay_edge(b) for b in range(4)])
-        for i in range(2):
-            arrived(og_all.at[2 * x + i, block_rows(y, outer_z), :], l_far.at[i])
+        arrived(pair(block_rows(y, outer_z)), l_far.at[0])
         start([relay_outer(b) for b in range(4)])
         start(saved_home())
         for kind, part in order:
-            arrived(w_slot(kind, outer_z, part), r_w.at[w_sem(kind, 2, part)])
+            arrived(w_slot(kind, outer_z, part), r_w.at[landing[kind, part]])
             start(w_relay(kind, part))
 
     @pl.when(is_worker)
     def _():
+        lane = 128
         start(grad_edge())
         start(saved_edge())
         start([w_mid(k, p) for k, p in order[:PARTS]])
-        pltpu.make_async_copy(og, og_all.at[t, block_rows(y, z), :], r_og.at[y * 4 + t]).start()
+        pltpu.make_async_copy(og, og_all.at[t, block_rows(y, z), :], r_og.at[0]).start()
         for block in range(4):
 
             @pl.when(block != t)
@@ -379,12 +383,15 @@
                 grad_own(block).start()
 
         slot = block_rows(y, z)
-        pltpu.make_async_copy(gl, gl_all.at[slot, :], r_gl.at[y * 3]).start()
-        pltpu.make_async_copy(ul, ul_all.at[slot, :], r_ul.at[y * 3]).start()
-        for kind, part in order:
-            pltpu.make_async_copy(
-                w_src(kind, part), w_slot(kind, z, part), r_w.at[w_sem(kind, 0, part)]
-            ).start()
+        pltpu.make_async_copy(gl, gl_all.at[slot, :], r_saved.at[y]).start()
+        pltpu.make_async_copy(ul, ul_all.at[slot, :], r_saved.at[y]).start()
+        pltpu.make_async_copy(dw, wd.at[z], r_w.at[DOWN_OWN]).start()
+        pltpu.make_async_copy(gw, wg.at[z], r_w.at[BOTH_OWN]).start()
+        pltpu.make_async_copy(uw, wu.at[z], r_w.at[BOTH_OWN]).start()
+
+        taps_src = cw.at[:, pl.ds(pl.multiple_of(t * hid, lane), hid)]
+        taps_copy = pltpu.make_async_copy(taps_src, taps_own, l_taps.at[0])
+        taps_copy.start()
 
         for rep in range(2):
             first = rep * n_rows + (z - 1) * (EDGE + 2 * rows)
@@ -396,13 +403,7 @@
         act[...] = jnp.zeros_like(act)
         conv_own[...] = jnp.zeros_like(conv_own)
 
-        for rep in range(2):
-            for block in range(4):
-                arrived(og_all.at[block, block_rows(rep, z), :], r_og.at[rep * 4 + block])
-            for i in range(2):
-                two = pl.ds(2 * i, 2)
-                arrived(og_all.at[two, edge_rows(rep, z), :], r_edge.at[rep * 2 + i])
-                arrived(og_all.at[two, block_rows(rep, outer_z), :], r_far.at[rep * 2 + i])
+        arrived(og_bytes(8 * (2 * rows + EDGE)), r_og.at[0])
 
         def level_of(role):
             near = jnp.where(role % 2 == 0, z, mid_z)
@@ -425,26 +426,23 @@
 
         def act_step(role, carry):
             level = level_of(role)
-            for part in range(PARTS):
-                arrived(w_slot(0, level, part), r_w.at[w_sem(0, role, part)])
+            arrived(wd.at[level], r_w.at[DOWN_OWN + role])
             act_product(level)
             return carry
 
         lax.fori_loop(0, 2, act_step, 0)
-        arrived(w_slot(0, 3 - outer_z, PARTS - 2), r_w.at[w_sem(0, 3, PARTS - 2)])
+        size = hid // PARTS
+        most = wd.at[3 - outer_z, pl.ds(0, hid - size), :]
+        arrived(most, r_w.at[DOWN_FAR])
         start([w_mid(k, p) for k, p in order[PARTS:]])
         act_step(2, 0)
-        for part in range(PARTS):
-            if part != PARTS - 2:
-                arrived(w_slot(0, 3 - outer_z, part), r_w.at[w_sem(0, 3, part)])
+        arrived(wd.at[3 - outer_z, pl.ds(hid - size, size), :], r_w.at[DOWN_LAST])
         act_product(3 - outer_z)
-
-        lane = 128
 
         def tile_step(rep, i):
             span = pl.ds(pl.multiple_of(rep * n_rows, EDGE), n_rows)
             cols = pl.ds(pl.multiple_of(i * lane, lane), lane)
-            taps = cw[:, pl.ds(pl.multiple_of(t * hid + i * lane, lane), lane)].astype(f32)
+            taps = taps_own[:, cols].astype(f32)
             own = gl_all[span, cols].astype(f32)
             before = pltpu.roll(own, 1, 0)
             behind = pltpu.roll(own, n_rows - 1, 0)
@@ -464,12 +462,10 @@
                     gate_grad[kept] * other[kept], axis=0, keepdims=True
                 )
 
+        taps_copy.wait()
         for turn in range(2):
             rep = 1 - y if turn == 0 else y
-            slots = (block_rows(rep, z), block_rows(rep, outer_z), edge_rows(rep, z))
-            for kind, slot in enumerate(slots):
-                arrived(gl_all.at[slot, :], r_gl.at[rep * 3 + kind])
-                arrived(ul_all.at[slot, :], r_ul.at[rep * 3 + kind])
+            arrived(saved_bytes(2 * (2 * rows + EDGE)), r_saved.at[rep])
 
             def turn_step(i, carry, rep=rep):
                 tile_step(rep, i)
@@ -493,133 +489,134 @@
                         kept, k * step_cols : (k + 1) * step_cols
                     ]
             for rep in range(2):
-                for half in range(2):
-                    away = to_other(rep, half, level)
-
-                    @pl.when(away)
-                    def _(rep=rep, half=half):
-                        for k in range(count):
-                            part_send(rep, half, level, first + k).start()
-
-                    @pl.when(jnp.logical_not(away))
-                    def _(rep=rep, half=half):
-                        for k in range(count):
-                            parts_in[t, first + k] = stage[
-                                rep, level, first + k, pl.ds(half * rows, rows), :
-                            ]
-
-        def wait_w(kind, role, level, part):
-            slot = pl.ds(pl.multiple_of(part * step_cols, step_cols), step_cols)
-            buffer = (wg, wu)[kind - 1]
-            arrived(buffer.at[level, slot, :], r_w.at[w_sem(kind, role, part)])
+                hand_on(rep, level, first, count)
+
+        def hand_on(rep, level, first, count):
+            for half in range(2):
+                away = to_other(rep, half, level)
+
+                @pl.when(away)
+                def _(half=half):
+                    for k in range(count):
+                        part_send(rep, half, level, first + k).start()
+
+                @pl.when(jnp.logical_not(away))
+                def _(half=half):
+                    for k in range(count):
+                        parts_in[t, first + k] = stage[
+                            rep, level, first + k, pl.ds(half * rows, rows), :
+                        ]
+
+        def rep_product(side, weight, level, slot, piece, rep):
+            kept = pl.ds(pl.multiple_of(rep * n_rows + EDGE, EDGE), 2 * rows)
+            return rows_dot(side[kept, piece], weight[level, slot, piece])
 
         def double_step(i, carry):
-            role, first = i // 2, 2 * (i % 2)
-            level = level_of(role)
-            for k in range(2):
-                for kind in (1, 2):
-                    wait_w(kind, role, level, first + k)
+            level, first = level_of(i // 2), 2 * (i % 2)
             total = product(lin_all, wg, level, first, 2) + product(up_all, wu, level, first, 2)
             emit(total, level, first, 2)
             return carry
 
+        arrived(wg.at[pl.ds(0, 2)], r_w.at[BOTH_OWN])
         lax.fori_loop(0, 2, double_step, 0)
 
         handed = remote(conv_own, conv_mid, s_mid.at[0], r_mid.at[0], (y, mid_z, t))
         handed.start()
+        arrived(wg.at[pl.ds(0, 2)], r_w.at[BOTH_NEAR])
         lax.fori_loop(2, 4, double_step, 0)
         arrived(conv_mid, r_mid.at[0])
         conv_all[t] = conv_own[...] + conv_mid[...]
+        arrived(wg.at[outer_z], r_w.at[BOTH_OUTER])
         lax.fori_loop(4, 5, double_step, 0)
         start(conv_sends())
+        arrived(wg.at[outer_z], r_w.at[BOTH_OUTER + 1])
         lax.fori_loop(5, 6, double_step, 0)
 
+        far = 3 - outer_z
+        every = pl.ds(0, hid)
+        ends = (pl.ds(0, cut), pl.ds(cut, hid - cut))
+
+        def far_step(part, pieces):
+            sem = BOTH_FAR + 2 * part
+            slot = pl.ds(part * step_cols, step_cols)
+            if not isinstance(part, int):
+                slot = pl.ds(pl.multiple_of(part * step_cols, step_cols), step_cols)
+            arrived(wg.at[far, slot, :], r_w.at[sem])
+            totals = [rep_product(lin_all, wg, far, slot, every, r) for r in (1 - y, y)]
+            for i, piece in enumerate(pieces):
+                arrived(wu.at[far, slot, piece], r_w.at[sem + 1 + i])
+                for turn, rep in enumerate((1 - y, y)):
+                    totals[turn] += rep_product(up_all, wu, far, slot, piece, rep)
+                    if i == len(pieces) - 1:
+                        stage[rep, far, part] = totals[turn].astype(bf16)
+                        hand_on(rep, far, part, 1)
+
         def single_step(part, carry):
-            level = level_of(3)
-            wait_w(1, 3, level, part)
-            total = product(lin_all, wg, level, part, 1)
-            wait_w(2, 3, level, part)
-            emit(total + product(up_all, wu, level, part, 1), level, part, 1)
+            far_step(part, (every,))
             return carry
 
-        lax.fori_loop(0, PARTS, single_step, 0)
-        sent([handed])
-
-    def remote_block(block):
-        return jnp.logical_not(jnp.logical_and(is_worker, t == block))
-
-    for block in range(4):
-
-        @pl.when(remote_block(block))
-        def _(block=block):
-            arrived(conv_all.at[block], r_conv.at[block])
-
-        cg[:, pl.ds(block * hid, hid)] = conv_all[block, 0:3, :]
+        lax.fori_loop(0, PARTS - 1, single_step, 0)
+        far_step(PARTS - 1, ends)
+        handed.wait_send()
 
     step_cols = width // PARTS
-    for part in range(PARTS):
-        for block in range(4):
-
-            @pl.when(remote_block(block))
-            def _(block=block):
-                arrived(parts_in.at[block, part], r_out.at[block * PARTS + part])
-
+
+    def add_up(part):
         total = parts_in[0, part].astype(f32)
         for block in range(1, 4):
             total = total + parts_in[block, part].astype(f32)
         out[:, part * step_cols : (part + 1) * step_cols] = total.astype(out.dtype)
 
+    def hear(buffer, sem):
+        @pl.when(is_worker)
+        def _():
+            arrived(buffer.at[pl.ds(0, 3)], sem)
+
+        @pl.when(jnp.logical_not(is_worker))
+        def _():
+            arrived(buffer, sem)
+
+    hear(conv_all, r_conv.at[0])
+    for block in range(4):
+        cg[:, pl.ds(block * hid, hid)] = conv_all[block, 0:3, :]
+
+    hear(parts_in.at[:, pl.ds(0, PARTS - 1)], r_out.at[0])
+    for part in range(PARTS - 1):
+        add_up(part)
+    hear(parts_in.at[:, PARTS - 1], r_out.at[1])
+    add_up(PARTS - 1)
+
     @pl.when(is_outer)
     def _():
-        sent(grad_outer())
+        arrived(og_bytes(rows), s_edge.at[0])
 
         @pl.when(lead)
         def _():
-            sent([w_outer(k, p) for k, p in order])
-            sent(saved_onward())
-            sent(saved_home())
+            arrived(wd.at[pl.ds(0, 3)], s_w.at[0])
+            arrived(saved_bytes(4 * rows), s_saved.at[0])
 
         @pl.when(core != y)
         def _():
-            sent(saved_across())
+            arrived(saved_bytes(2 * rows), s_saved.at[0])
+
+    @pl.when(inner)
+    def _():
+        arrived(og_bytes(EDGE), s_edge.at[0])
+        arrived(wd.at[pl.ds(0, 3)], s_w.at[0])
 
     @pl.when(is_relay)
     def _():
-        sent(grad_edge())
-        sent(saved_edge())
-        sent([grad_own(b) for b in range(4)])
-        sent(saved_home())
-        sent([relay_edge(b) for b in range(4)])
-        sent([relay_outer(b) for b in range(4)])
-        for kind, part in order:
-            sent(w_relay(kind, part))
+        arrived(og_bytes(4 * rows), s_og.at[0])
+        arrived(og_bytes(8 * (rows + EDGE)), s_far.at[0])
+        arrived(saved_bytes(2 * (rows + EDGE)), s_saved.at[0])
+        arrived(wd.at[pl.ds(0, 3)], s_w.at[1])
 
     @pl.when(is_worker)
     def _():
-        sent(grad_edge())
-        sent(saved_edge())
-        sent([w_mid(k, p) for k, p in order])
-        for block in range(4):
-
-            @pl.when(block != t)
-            def _(block=block):
-                grad_own(block).wait_send()
-
-        sent(conv_sends())
-
-        def done_step(i, carry):
-            block, part = i // PARTS, i % PARTS
-            for rep in range(2):
-                for half in range(2):
-
-                    @pl.when(to_other(rep, half, block))
-                    def _(rep=rep, half=half):
-                        part_send(rep, half, block, part).wait_send()
-
-            return carry
-
-        lax.fori_loop(0, 4 * PARTS, done_step, 0)
-
+        arrived(og_bytes(3 * rows), s_og.at[0])
+        arrived(saved_bytes(2 * EDGE), s_saved.at[0])
+        arrived(act.at[pl.ds(0, 15 * 8), :], s_conv.at[0])
+        arrived(og_bytes(15 * rows), s_out.at[0])
 
 def fused(out_grad, gate_lin, up_lin, conv_weight, gate_weight, up_weight, down_weight):
     f32, bf16 = jnp.float32, jnp.bfloat16
@@ -627,15 +624,15 @@
     hid = gate_lin.shape[1]
     n_rows = 2 * rows + 2 * EDGE
     dma = pltpu.SemaphoreType.DMA
-    hbm = pl.BlockSpec(memory_space=pl.ANY)
+    hbm = pl.BlockSpec(memory_space=pltpu.HBM)
     vmem = pl.BlockSpec(memory_space=pltpu.VMEM)
-    return pl.pallas_call(
+    held = pl.pallas_call(
         kernel,
         out_shape=(
             jax.ShapeDtypeStruct((rows, width), bf16),
             jax.ShapeDtypeStruct((3, 4 * hid), f32),
         ),
-        in_specs=[hbm, hbm, hbm, vmem, hbm, hbm, hbm],
+        in_specs=[hbm] * 7,
         out_specs=(vmem, vmem),
         scratch_shapes=[
             pltpu.VMEM((4, 2 * n_rows, width), bf16),
@@ -649,16 +646,36 @@
             pltpu.VMEM((4, width, hid), bf16),
             pltpu.VMEM((2, 4, PARTS, 2 * rows, width // PARTS), bf16),
             pltpu.VMEM((4, PARTS, rows, width // PARTS), bf16),
+            pltpu.VMEM((3, hid), bf16),
             pltpu.VMEM((8, hid), f32),
             pltpu.VMEM((8, hid), f32),
             pltpu.VMEM((4, 8, hid), f32),
         ]
-        + [dma((n,)) for n in (8, 4, 4, 2, 2, 2, 6, 6, 12 * PARTS, 4 * PARTS, 1, 4)]
-        + [dma((n,)) for n in (4, 8, 1, 2, 2, 1, 12 * PARTS, 16 * PARTS, 1, 15)],
+        + [dma((n,)) for n in (1, 1, 1, 2, 1, 2, 18, 2, 1, 1)]
+        + [dma((n,)) for n in (1, 1, 1, 1, 2, 1, 1, 1)],
         compiler_params=pltpu.CompilerParams(
-            collective_id=0, has_side_effects=True, vmem_limit_bytes=67_000_000
+            collective_id=0, has_side_effects=True, vmem_limit_bytes=56_000_000
         ),
-    )(out_grad, gate_lin, up_lin, conv_weight, gate_weight, up_weight, down_weight)
+    )(out_grad, gate_lin, up_lin, pltpu.with_memory_space_constraint(conv_weight, pltpu.HBM), gate_weight, up_weight, down_weight)
+    return pl.pallas_call(
+        write_out,
+        out_shape=tuple(jax.ShapeDtypeStruct(a.shape, a.dtype) for a in held),
+        in_specs=[vmem] * 2,
+        out_specs=(hbm, hbm),
+        scratch_shapes=[dma((2,))],
+        compiler_params=pltpu.CompilerParams(vmem_limit_bytes=2_000_000),
+    )(*held)
+
+
+def write_out(first, second, first_out, second_out, sems):
+    copies = [
+        pltpu.make_async_copy(first, first_out, sems.at[0]),
+        pltpu.make_async_copy(second, second_out, sems.at[1]),
+    ]
+    for copy in copies:
+        copy.start()
+    for copy in copies:
+        copy.wait()
 
 
 def solution(mesh):

time: 116 us -> 109 us (0.940)
  local copies, waits for them, and re-layouts: 3.21 us -> 0 us
  Pallas kernels: 111 us -> 108 us
    pallas_call x1, Pallas kernels: 111 us -> 107 us  [fused(): pl.pallas_call(kernel, out_shape=(jax.ShapeDtypeStruct((rows, width), bf1...]
    unnamed x2 -> x0, local copies, waits for them, and re-layouts: 3.21 us -> none
where the time goes in v2:
time: 109 us
  Pallas kernels  108 us (99%)
    pallas_call x1, Pallas kernels, fused(): pl.pallas_call(kernel, out_shape=(jax.ShapeDtypeStruct((rows, width), bf1...  107 us

profile of v2, /device:TPU:3, one launch (start us, length us, event | category | flops | bytes accessed | tf_op | source)
XLA Modules:
  0.0 108.7 jit_solution(11546507432618174761)
XLA Ops:
  0.6 107.1 %shard_map.86 = (bf16[256,512]{1,0:T(8,128)(2,1)S(1)}, f32[3,5632]{1,0:T(4,128)S(1)}) custom-call(bf16[256,512]{1,0:T(8,128)(2,1)} %og.1, bf16[256,1408]{1,0:T(8,128)(2,1)} %gl.1, bf16[256,1408]{1,0:T(8,128)(2,1)} %ul.1, bf16[3,5632]{1,0:T(4,128)(2,1)} %cw.1, bf16[512,1408]{1,0:T(8,128)(2,1)} %gw.1, bf16[512,1408]{1,0:T(8,128)(2,1)} %uw.1, bf16[1408,512]{1,0:T(8,128)(2,1)} %dw.1), custom_call_target="tpu_custom_call" | custom-call | tf_op jit(solution)/shard_map/pallas_call | solution.py:629
  107.8 0.7 shard_map.87
